TPU v7x, 32 devices: a whole 2x2x4 slice. The times are simulated.
32 devices in a mesh: grp: 2 (over y), fs: 4 (over z), tp: 4 (over x, core).
Axes of the slice: x: 2, y: 2, z: 4, core: 2. Of those that a mesh axis runs over, the one named last changes fastest.
Arguments:
- tokens: bfloat16 [3072, 2048], P(('grp', 'fs')), parts along dimension 0, may hold values from -3 to 3
- gate_weight: bfloat16 [2048, 5120], P('fs', 'tp'), may hold values from -0.125 to 0.125
- up_weight: bfloat16 [2048, 5120], P('fs', 'tp'), may hold values from -0.125 to 0.125
- down_weight: bfloat16 [5120, 2048], P('tp', 'fs'), may hold values from -0.078125 to 0.078125
- pool_weight: bfloat16 [512, 4, 512], P('fs', None, 'tp'), may hold values from -0.375 to 0.375
- pool_bias: float32 [4, 512], replicated, may hold values from -3 to 3
- pool_scale: float32 [2048], replicated, may hold values from 0.1 to 1.9
- gain_first: float32 [2048], replicated, may hold values from 0.1 to 1.9
- gain_mix: float32 [2048], replicated, may hold values from 0.1 to 1.9
- gain_second: float32 [2048], replicated, may hold values from 0.1 to 1.9
Outputs:
- result: bfloat16 [3072, 2048], P(('grp', 'fs')), parts along dimension 0
There are 2 independent parts, one for each index of `grp`. A program takes and returns all parts, laid end to end along the dimension named above; an argument that names none is the same for every part. Nothing has to cross between parts.
All inputs are finite; a program needn't handle non-finite values.
Results may differ from a plain program's by a relative error of at most 0.018.
Values may be sent and summed in bfloat16 or wider, within the bound.
A program may use at most 64 MiB of HBM per device.

v0:
```python
import jax
import jax.numpy as jnp
from jax import lax
from jax.sharding import PartitionSpec as P

eps = 1e-06
pool_spans = (2, 4, 8, 16)
pad_width = 8


def rms_scale(values, gain_vec):
    fvalues = values.astype(jnp.float32)
    scaled = fvalues * lax.rsqrt(jnp.mean(fvalues * fvalues, axis=-1, keepdims=True) + eps)
    return (scaled * gain_vec).astype(jnp.bfloat16)


def ffn_hidden(normed, gate_full, up_full):
    gate_proj = jnp.dot(normed, gate_full, preferred_element_type=jnp.float32)
    up_proj = jnp.dot(normed, up_full, preferred_element_type=jnp.float32)
    return (jax.nn.silu(gate_proj) * up_proj).astype(jnp.bfloat16)


def pool_block(padded, offset, seq_len, pool_full, pool_bias, pool_scale):
    n_tokens = padded.shape[0] - 2 * pad_width
    group_width = pool_full.shape[0]
    position = offset + lax.iota(jnp.int32, n_tokens)
    column_pos = offset - pad_width + lax.iota(jnp.int32, padded.shape[0])
    center = padded[pad_width : pad_width + n_tokens].astype(jnp.float32)
    outputs = []
    for group_number, window_span in enumerate(pool_spans):
        low_edge = jnp.clip(position - window_span // 2, 0, seq_len)
        high_edge = jnp.clip(position - window_span // 2 + window_span, 0, seq_len)
        band_mask = (
            (column_pos[None, :] >= low_edge[:, None]) & (column_pos[None, :] < high_edge[:, None])
        ).astype(jnp.bfloat16)
        lower_col = group_number * group_width
        columns = padded[:, lower_col : lower_col + group_width]
        window_sum = jnp.dot(band_mask, columns, preferred_element_type=jnp.float32)
        window_mean = window_sum / (high_edge - low_edge).astype(jnp.float32)[:, None]
        deviation = (window_mean - center[:, lower_col : lower_col + group_width]).astype(
            jnp.bfloat16
        )
        mapped = jnp.dot(
            deviation, pool_full[:, group_number, :], preferred_element_type=jnp.float32
        )
        outputs.append(mapped + pool_bias[group_number])
    return jnp.concatenate(outputs, axis=-1) * pool_scale


def shards(
    tokens,
    gate_weight,
    up_weight,
    down_weight,
    pool_weight,
    pool_bias,
    pool_scale,
    gain_first,
    gain_mix,
    gain_second,
):
    gate_full, up_full, pool_half = (
        lax.all_gather(gate_weight, "fs", axis=0, tiled=True),
        lax.all_gather(up_weight, "fs", axis=0, tiled=True),
        lax.all_gather(pool_weight, "fs", axis=0, tiled=True),
    )
    down_full = lax.all_gather(down_weight, "fs", axis=1, tiled=True)
    pool_full = lax.all_gather(pool_half, "tp", axis=2, tiled=True)
    seq_len = tokens.shape[0]
    first_normed = rms_scale(tokens, gain_first)
    first_hidden = ffn_hidden(first_normed, gate_full, up_full)
    second_gate, second_up, second_down = (gate_full, up_full, down_full)
    first_branch = lax.psum(
        jnp.dot(first_hidden, down_full, preferred_element_type=jnp.float32).astype(jnp.bfloat16),
        "tp",
    ).astype(jnp.float32)
    after_first = (tokens.astype(jnp.float32) + 0.5 * first_branch).astype(jnp.bfloat16)
    mix_normed = rms_scale(after_first, gain_mix)
    padded = jnp.pad(mix_normed, ((pad_width, pad_width), (0, 0)))
    mixed = pool_block(padded, 0, seq_len, pool_full, pool_bias, pool_scale)
    after_mix = (after_first.astype(jnp.float32) + mixed).astype(jnp.bfloat16)
    second_normed = rms_scale(after_mix, gain_second)
    second_hidden = ffn_hidden(second_normed, second_gate, second_up)
    second_branch = lax.psum(
        jnp.dot(second_hidden, second_down, preferred_element_type=jnp.float32).astype(
            jnp.bfloat16
        ),
        "tp",
    ).astype(jnp.float32)
    return (after_mix.astype(jnp.float32) + 0.5 * second_branch).astype(jnp.bfloat16)


def solution(mesh):
    return jax.shard_map(
        shards,
        mesh=mesh,
        in_specs=(
            P(("grp", "fs"), None),
            P("fs", "tp"),
            P("fs", "tp"),
            P("tp", "fs"),
            P("fs", None, "tp"),
            P(),
            P(),
            P(),
            P(),
            P(),
        ),
        out_specs=P(("grp", "fs"), None),
        check_vma=False,
    )
```

profile of v0, /device:TPU:1, one launch (start us, length us, event | category | flops | bytes accessed | tf_op | source)
XLA Modules:
  0.0 467.5 jit_solution(4957366809883981244)
XLA Ops:
  6.5 0.0 copy-start
  6.5 0.0 copy-start.8
  6.5 0.0 all-gather.5.cloned.1.call-start
  6.5 0.7 all-gather.5.cloned.1.call-update
  7.3 0.0 all-gather.7.cloned.1.call-start
  7.3 0.7 all-gather.7.cloned.1.call-update
  8.0 0.0 all-gather.9.cloned.1.call-start
  8.1 0.7 all-gather.9.cloned.1.call-update
  8.7 0.0 all-reduce.4.cloned.1.call-start
  8.8 0.0 copy-done
  8.8 0.4 fusion
  9.2 99.9 %all-gather.5.cloned.1.call-done = bf16[2048,1280]{1,0:T(8,128)(2,1)} async-done(((bf16[512,1280]{1,0:T(8,128)(2,1)}), bf16[2048,1280]{1,0:T(8,128)(2,1)}) %all-gather.5.cloned.1.call-update) | async-done | bytes 5242896 | tf_op jit(solution)/shard_map/all_gather | solution.py:63
  109.1 0.0 copy-done.8
  109.1 6.0 %fusion.56 = f32[384,1280]{1,0:T(8,128)} fusion(bf16[2048,1280]{1,0:T(8,128)(2,1)} %all-gather.5.cloned.1.call-done, bf16[384,2048]{1,0:T(8,128)(2,1)S(1)} %copy-done, f32[2048]{0:T(1024)S(1)} %copy-done.8, f32[384]{0:T(512)S(1)} %add_rsqrt_fusion.2), kind=kOutput, calls=%fused_computation.69 | convolution fusion | flops 2016411648 | bytes 8791552 | tf_op jit(solution)/shard_map/dot_general | solution.py:18
  115.1 0.0 copy-start.4
  115.1 0.0 copy-start.7
  115.1 92.0 %all-gather.7.cloned.1.call-done = bf16[2048,1280]{1,0:T(8,128)(2,1)} async-done(((bf16[512,1280]{1,0:T(8,128)(2,1)}), bf16[2048,1280]{1,0:T(8,128)(2,1)}) %all-gather.7.cloned.1.call-update) | async-done | bytes 5242896 | tf_op jit(solution)/shard_map/all_gather | solution.py:64
  207.0 98.0 %all-gather.9.cloned.1.call-done = bf16[1280,2048]{1,0:T(8,128)(2,1)} async-done(((bf16[1280,512]{1,0:T(8,128)(2,1)}), bf16[1280,2048]{1,0:T(8,128)(2,1)}) %all-gather.9.cloned.1.call-update) | async-done | bytes 5242896 | tf_op jit(solution)/shard_map/all_gather | solution.py:67
  305.0 10.6 %convolution_convert_fusion.1 = bf16[384,2048]{1,0:T(8,128)(2,1)} fusion(bf16[1280,2048]{1,0:T(8,128)(2,1)} %all-gather.9.cloned.1.call-done, bf16[2048,1280]{1,0:T(8,128)(2,1)} %all-gather.7.cloned.1.call-done, f32[384,1280]{1,0:T(8,128)} %fusion.56, bf16[384,2048]{1,0:T(8,128)(2,1)S(1)} %copy-done, f32[2048]{0:T(1024)S(1)} %copy-done.8, ...), kind=kOutput, calls=%fused_computation.25 | convolution fusion | flops 4033413120 | bytes 15607296 | tf_op jit(solution)/shard_map/dot_general | solution.py:74
  315.6 0.0 copy-start.5
  315.6 0.0 all-reduce.4.cloned.1.call-update
  315.7 0.0 all-gather.11.cloned.1.call-start
  315.7 0.0 copy-done.4
  315.8 13.0 %all_gather.18 = bf16[512,4,128]{2,0,1:T(8,128)(2,1)} all-gather(bf16[128,4,128]{2,0,1:T(8,128)(2,1)S(1)} %copy.11), channel_id=1, replica_groups=mesh['grp'=2,'fs'=4,'tp'=4] {'fs'}, dimensions={0}, use_global_device_ids=true | all-gather | bytes 655360 | tf_op jit(solution)/shard_map/all_gather | solution.py:65
  328.8 0.0 all-gather.11.cloned.1.call-update
  328.8 0.2 all-reduce.6.cloned.1.call-start
  329.1 0.0 copy-done.7
  329.2 27.7 %all-reduce.4.cloned.1.call-done = bf16[384,2048]{1,0:T(8,128)(2,1)} async-done(((bf16[384,2048]{1,0:T(8,128)(2,1)}), bf16[384,2048]{1,0:T(8,128)(2,1)}) %all-reduce.4.cloned.1.call-update) | async-done | bytes 1572880 | tf_op jit(solution)/shard_map/psum | solution.py:73
  356.9 0.0 copy-start.1
  356.9 2.2 fusion.4
  359.1 0.0 copy-done.5
  359.1 0.0 copy-done.1
  359.1 3.0 fusion.97
  362.1 19.6 %all-gather.11.cloned.1.call-done = bf16[512,4,512]{2,0,1:T(8,128)(2,1)} async-done(((bf16[512,4,128]{2,0,1:T(8,128)(2,1)}), bf16[512,4,512]{2,0,1:T(8,128)(2,1)}) %all-gather.11.cloned.1.call-update) | async-done | bytes 2097168 | tf_op jit(solution)/shard_map/all_gather | solution.py:68
  381.7 3.0 convolution_add_fusion
  384.7 3.0 convolution_add_fusion.1
  387.7 3.0 convolution_add_fusion.2
  390.7 0.0 copy-start.6
  390.7 3.0 convolution_add_fusion.3
  393.7 0.0 copy-done.6
  393.7 0.0 copy-start.9
  393.7 2.9 fusion.8
  396.6 0.0 copy-start.2
  396.6 1.1 copy-done.2
  397.7 0.0 copy-done.9
  397.7 6.0 %fusion.52 = f32[384,1280]{1,0:T(8,128)} fusion(bf16[2048,1280]{1,0:T(8,128)(2,1)} %all-gather.5.cloned.1.call-done, bf16[384,2048]{1,0:T(8,128)(2,1)S(1)} %get-tuple-element.6, f32[2048]{0:T(1024)S(1)} %copy-done.9, f32[384]{0:T(512)S(1)} %add_rsqrt_fusion), kind=kOutput, calls=%fused_computation.68 | convolution fusion | flops 2016411648 | bytes 8791552 | tf_op jit(solution)/shard_map/dot_general | solution.py:18
  403.7 0.0 copy-start.3
  403.7 11.2 %convolution_convert_fusion = bf16[384,2048]{1,0:T(8,128)(2,1)} fusion(bf16[1280,2048]{1,0:T(8,128)(2,1)} %all-gather.9.cloned.1.call-done, bf16[2048,1280]{1,0:T(8,128)(2,1)} %all-gather.7.cloned.1.call-done, f32[384,1280]{1,0:T(8,128)} %fusion.52, bf16[384,2048]{1,0:T(8,128)(2,1)} %copy-done.2, f32[2048]{0:T(1024)S(1)} %copy-done.9, f32[384]{0:T(512)S(1)} %add_rsqrt_fusion), kind=kOutput, calls=%fused_computation.24 | convolution fusion | flops 4033413120 | bytes 15607296 | tf_op jit(solution)/shard_map/dot_general | solution.py:85
  414.9 0.0 all-reduce.6.cloned.1.call-update
  415.0 42.5 %all-reduce.6.cloned.1.call-done = bf16[384,2048]{1,0:T(8,128)(2,1)} async-done(((bf16[384,2048]{1,0:T(8,128)(2,1)}), bf16[384,2048]{1,0:T(8,128)(2,1)}) %all-reduce.6.cloned.1.call-update) | async-done | bytes 1572880 | tf_op jit(solution)/shard_map/psum | solution.py:84
  457.4 0.0 copy-done.3
  457.4 3.2 fusion.11
  (14 shorter events, 0.1 us)
Async XLA Ops:
  6.5 2.3 copy-start
  6.5 102.5 %copy-start.8 = (f32[2048]{0:T(1024)S(1)}, f32[2048]{0:T(1024)}, u32[]{:S(2)}) copy-start(f32[2048]{0:T(1024)} %param.17) | copy-start | bytes 24580
  6.5 102.5 %all-gather.5.cloned.1.call-start = ((), (), s32[]{:S(2)}) async-start(), calls=%async_computation | async-start | bytes 6553600 | tf_op jit(solution)/shard_map/all_gather | solution.py:63
  7.3 199.8 %all-gather.7.cloned.1.call-start = ((), (), s32[]{:S(2)}) async-start(), calls=%async_computation.1 | async-start | bytes 6553600 | tf_op jit(solution)/shard_map/all_gather | solution.py:64
  8.0 297.0 %all-gather.9.cloned.1.call-start = ((), (), s32[]{:S(2)}) async-start(), calls=%async_computation.2 | async-start | bytes 6553600 | tf_op jit(solution)/shard_map/all_gather | solution.py:67
  8.7 348.1 %all-reduce.4.cloned.1.call-start = ((), (), s32[]{:S(2)}) async-start(), calls=%async_computation.3 | async-start | bytes 3145728 | tf_op jit(solution)/shard_map/psum | solution.py:73
  115.1 200.7 %copy-start.4 = (bf16[128,4,128]{2,1,0:T(4,128)(2,1)S(1)}, bf16[128,4,128]{2,1,0:T(4,128)(2,1)}, u32[]{:S(2)}) copy-start(bf16[128,4,128]{2,1,0:T(4,128)(2,1)} %param.14) | copy-start | bytes 393220
  115.1 214.1 %copy-start.7 = (f32[4,512]{1,0:T(4,128)S(1)}, f32[4,512]{1,0:T(4,128)}, u32[]{:S(2)}) copy-start(f32[4,512]{1,0:T(4,128)} %param.15) | copy-start | bytes 24580
  315.6 43.5 %copy-start.5 = (f32[2048]{0:T(1024)S(1)}, f32[2048]{0:T(1024)}, u32[]{:S(2)}) copy-start(f32[2048]{0:T(1024)} %param.18) | copy-start | bytes 24580
  315.7 66.0 %all-gather.11.cloned.1.call-start = ((), (), s32[]{:S(2)}) async-start(), calls=%async_computation.4 | async-start | bytes 2621440 | tf_op jit(solution)/shard_map/all_gather | solution.py:68
  328.8 128.6 %all-reduce.6.cloned.1.call-start = ((), (), s32[]{:S(2)}) async-start(), calls=%async_computation.5 | async-start | bytes 3145728 | tf_op jit(solution)/shard_map/psum | solution.py:84
  356.9 2.2 copy-start.1
  390.7 3.0 copy-start.6
  393.7 4.1 copy-start.9
  396.6 1.1 copy-start.2
  403.7 53.7 %copy-start.3 = (bf16[384,2048]{1,0:T(8,128)(2,1)S(1)}, bf16[384,2048]{1,0:T(8,128)(2,1)}, u32[]{:S(2)}) copy-start(bf16[384,2048]{1,0:T(8,128)(2,1)} %copy-done.2) | copy-start | bytes 4718596
Sparse Core Ops, SparseCore 0:
  8.9 100.1 all-gather.4
  110.6 96.3 all-gather.6
  208.6 96.3 all-gather.8
  315.8 41.0 all-reduce.3
  358.3 23.3 all-gather.10
  415.1 42.3 all-reduce.5
where the time goes:
time: 469 us; the launch traced here: 467 us
  waiting for transfers between devices  382 us (81%)
  matrix products  45.8 us (10%)
  between operations  13.6 us (3%)
  blocking collectives  13 us (3%)
  other arithmetic  11.8 us (3%)
    all_gather x1, waiting for transfers between devices, shards(): lax.all_gather(gate_weight, 'fs', axis=0, tiled=True)  99.9 us
    all_gather x1, waiting for transfers between devices, shards(): down_full = lax.all_gather(down_weight, 'fs', axis=1, tiled=True)  98 us
    all_gather x1, waiting for transfers between devices, shards(): lax.all_gather(up_weight, 'fs', axis=0, tiled=True)  92 us
    psum x1, waiting for transfers between devices, shards(): lax.psum(jnp.dot(second_hidden, second_down, preferred_element_type=jnp.f...  42.5 us
    psum x1, waiting for transfers between devices, shards(): lax.psum(jnp.dot(first_hidden, down_full, preferred_element_type=jnp.floa...  27.7 us
    all_gather x1, waiting for transfers between devices, shards(): pool_full = lax.all_gather(pool_half, 'tp', axis=2, tiled=True)  19.6 us
    all_gather x1, blocking collectives, shards(): lax.all_gather(pool_weight, 'fs', axis=0, tiled=True)  13 us
    dot_general x2, matrix products, ffn_hidden(): gate_proj = jnp.dot(normed, gate_full, preferred_element_type=jnp.float32)  12 us
  transfers between devices with their start and end apart: 6, of which 6 were waited for; matrix products, arithmetic and copies ran while one was open for 3% of the time, Pallas kernels for 0%

commit v1 on v0

--- a/solution.py
+++ b/solution.py
@@ -1,11 +1,16 @@
+import functools
+
 import jax
 import jax.numpy as jnp
 from jax import lax
+from jax.experimental import pallas as pl
+from jax.experimental.pallas import tpu as pltpu
 from jax.sharding import PartitionSpec as P
 
 eps = 1e-06
 pool_spans = (2, 4, 8, 16)
 pad_width = 8
+MESH = pl.DeviceIdType.MESH
 
 
 def rms_scale(values, gain_vec):
@@ -90,9 +95,393 @@
     return (after_mix.astype(jnp.float32) + 0.5 * second_branch).astype(jnp.bfloat16)
 
 
+def fused_kernel(
+    sizes, tok_ref, gate_ref, up_ref, down_ref, pool_ref, bias_ref, scale_ref, gain1_ref, gainm_ref, gain2_ref,
+    out_ref,
+    gu_full, down_full, pool_full, acc, normed, hidden, amix, res, part, rbuf, xs, xr,
+    zsend, zleft, zrecv, ysend, yrecv, tsend, trecv, lsem, csend, crecv, xsend, xrecv, fsend, frecv, osem,
+):
+    n, n_tp = sizes
+    g, z, t = lax.axis_index("grp"), lax.axis_index("fs"), lax.axis_index("tp")
+    core = lax.rem(t, 2)
+    y_peer, right, left = {"grp": 1 - g}, {"fs": z + 1}, {"fs": z - 1}
+    mate, x_peer = {"tp": t + 1 - 2 * core}, {"tp": lax.rem(t + 2, n_tp)}
+    n_rows, width = tok_ref.shape
+    d_loc, f_loc = gate_ref.shape
+    groups, pool_rows, pool_cols = pool_ref.shape
+    half_rows = n_rows // 2
+    f32 = jnp.float32
+
+    def remote(src, dst, s_sem, r_sem, dev):
+        return pltpu.make_async_remote_copy(
+            src_ref=src, dst_ref=dst, send_sem=s_sem, recv_sem=r_sem, device_id=dev, device_id_type=MESH
+        )
+
+    barrier = pltpu.get_barrier_semaphore()
+
+    def greet(dev):
+        pl.semaphore_signal(barrier, inc=1, device_id=dev, device_id_type=MESH)
+
+    greet(y_peer)
+    for off in range(1, n_tp):
+        greet({"tp": lax.rem(t + off, n_tp)})
+
+    @pl.when(z > 0)
+    def _():
+        greet(left)
+
+    @pl.when(z < n - 1)
+    def _():
+        greet(right)
+
+    pl.semaphore_wait(barrier, n_tp + jnp.minimum(z, 1) + jnp.minimum(n - 1 - z, 1))
+
+    pieces = [("pool", 0, 1)] + [(name, c, 2) for name in ("gate", "up", "down") for c in range(2)]
+    n_pieces = len(pieces)
+
+    def rows_of(name, half, c, count):
+        total = {"pool": pool_rows, "gate": d_loc, "up": d_loc, "down": f_loc}[name]
+        size = total // (2 * count)
+        return half * (total // 2) + c * size, size, total
+
+    def region(name, s, half, c, count):
+        start, size, total = rows_of(name, half, c, count)
+        if name == "down":
+            return down_full.at[s, pl.ds(pl.multiple_of(start, 16), size), :]
+        rows = pl.ds(pl.multiple_of(s * total + start, 16), size)
+        if name == "pool":
+            return pool_full.at[:, rows, pl.ds(pl.multiple_of(t * pool_cols, 128), pool_cols)]
+        return gu_full.at[0 if name == "gate" else 1, rows, :]
+
+    def source(name, half, c, count):
+        start, size, _ = rows_of(name, half, c, count)
+        rows = pl.ds(pl.multiple_of(start, 16), size)
+        if name == "pool":
+            return pool_ref.at[:, rows, :]
+        return {"gate": gate_ref, "up": up_ref, "down": down_ref}[name].at[rows, :]
+
+    def own_right(k):
+        name, c, count = pieces[k]
+        return remote(source(name, g, c, count), region(name, z, g, c, count), zsend.at[z, k], zrecv.at[z, k], right)
+
+    def own_left(k):
+        name, c, count = pieces[k]
+        return remote(source(name, g, c, count), region(name, z, g, c, count), zleft.at[k], zrecv.at[z, k], left)
+
+    def pass_on(k, s, dev):
+        name, c, count = pieces[k]
+        there = region(name, s, g, c, count)
+        return remote(there, there, zsend.at[s, k], zrecv.at[s, k], dev)
+
+    def share(k, s, half):
+        name, c, count = pieces[k]
+        there = region(name, s, half, c, count)
+        return remote(there, there, ysend.at[s, k], yrecv.at[s, k], y_peer)
+
+    for k in range(n_pieces):
+
+        @pl.when(z < n - 1)
+        def _():
+            own_right(k).start()
+
+        @pl.when(z > 0)
+        def _():
+            own_left(k).start()
+
+    own_rows = pl.ds(pl.multiple_of(z * d_loc, 128), d_loc)
+    own_pool = pool_full.at[
+        :, pl.ds(pl.multiple_of(z * pool_rows, 16), pool_rows), pl.ds(pl.multiple_of(t * pool_cols, 128), pool_cols)
+    ]
+    local = [
+        pltpu.make_async_copy(pool_ref, own_pool, lsem.at[0]),
+        pltpu.make_async_copy(gate_ref, gu_full.at[0, own_rows, :], lsem.at[1]),
+        pltpu.make_async_copy(up_ref, gu_full.at[1, own_rows, :], lsem.at[2]),
+        pltpu.make_async_copy(down_ref, down_full.at[z], lsem.at[3]),
+    ]
+    for copy in local:
+        copy.start()
+
+    def norm_rows(src, gain):
+        @pl.loop(0, n_rows // 32)
+        def _(r):
+            rows = pl.ds(pl.multiple_of(r * 32, 32), 32)
+            values = src[rows, :].astype(f32)
+            scaled = values * lax.rsqrt(jnp.mean(values * values, axis=-1, keepdims=True) + eps)
+            normed[rows, :] = (scaled * gain[...]).astype(jnp.bfloat16)
+
+    tile = 256
+
+    def add_shard(w, s):
+        k_cols = pl.ds(pl.multiple_of(s * d_loc, 128), d_loc)
+
+        @pl.loop(0, f_loc // tile)
+        def _(i):
+            cols = pl.ds(pl.multiple_of(i * tile, tile), tile)
+            acc[w, :, cols] += jnp.dot(normed[:, k_cols], gu_full[w, k_cols, cols], preferred_element_type=f32)
+
+    def pool_copy(off, s, sender):
+        cols = pl.ds(pl.multiple_of(sender * pool_cols, 128), pool_cols)
+        there = pool_full.at[:, pl.ds(pl.multiple_of(s * pool_rows, 16), pool_rows), cols]
+        return remote(there, there, tsend.at[off - 1, s], trecv.at[off - 1, s], {"tp": lax.rem(t + off, n_tp)})
+
+    def spread_pool(s):
+        for off in range(1, n_tp):
+            pool_copy(off, s, t).start()
+
+    norm_rows(tok_ref, gain1_ref)
+    acc[...] = jnp.zeros_like(acc)
+    for copy in local:
+        copy.wait()
+    spread_pool(z)
+
+    @pl.loop(0, 2)
+    def _(w):
+        add_shard(w, z)
+
+    def both_sides(d, act):
+        @pl.when(z >= d)
+        def _():
+            act(z - d, z < n - 1, right)
+
+        @pl.when(z + d < n)
+        def _():
+            act(z + d, z > 0, left)
+
+    def relay(name, d):
+        for k in range(n_pieces):
+            if pieces[k][0] != name:
+                continue
+
+            def act(s, more, dev):
+                pass_on(k, s, dev).wait_recv()
+
+                @pl.when(more)
+                def _():
+                    pass_on(k, s, dev).start()
+
+                share(k, s, g).start()
+
+            both_sides(d, act)
+
+    def settle(name, s):
+        for k in range(n_pieces):
+            if pieces[k][0] == name:
+                share(k, s, 1 - g).wait_recv()
+
+    def settle_pool(s, *_):
+        settle("pool", s)
+        spread_pool(s)
+
+    def settle_gate(s, *_):
+        settle("gate", s)
+        add_shard(0, s)
+
+    def settle_up(s, *_):
+        settle("up", s)
+        add_shard(1, s)
+
+    @pl.loop(1, n)
+    def _(d):
+        relay("pool", d)
+        relay("gate", d)
+        both_sides(d, settle_pool)
+        relay("up", d)
+        both_sides(d, settle_gate)
+        relay("down", d)
+        both_sides(d, settle_up)
+
+    def activate(gate_proj, up_proj):
+        return (gate_proj / (1.0 + jnp.exp(-gate_proj)) * up_proj).astype(jnp.bfloat16)
+
+    @pl.loop(0, f_loc // tile)
+    def _(i):
+        cols = pl.ds(pl.multiple_of(i * tile, tile), tile)
+        hidden[:, cols] = activate(acc[0, :, cols], acc[1, :, cols])
+
+    turn = 1 - 2 * ((2 * z) // n)
+    mine = pl.ds(pl.multiple_of(core * half_rows, 16), half_rows)
+    other = pl.ds(pl.multiple_of((1 - core) * half_rows, 16), half_rows)
+
+    def branch_sum(phase, base):
+        def block(j):
+            return lax.rem(z + turn * j + n, n)
+
+        def pair_copy(j):
+            return remote(part.at[phase, j, other, :], rbuf.at[phase, j], csend.at[phase, j], crecv.at[phase, j], mate)
+
+        def x_copy(j):
+            return remote(xs.at[phase, j], xr.at[phase, j], xsend.at[phase, j], xrecv.at[phase, j], x_peer)
+
+        def final_copy(j, rows):
+            there = res.at[phase, rows, pl.ds(pl.multiple_of(block(j) * d_loc, 128), d_loc)]
+            return remote(there, there, fsend.at[phase, j], frecv.at[phase, j], mate)
+
+        def multiply(j):
+            s = block(j)
+            if phase == 0 and j > 0:
+                settle("down", s)
+
+            @pl.loop(0, d_loc // tile)
+            def _(i):
+                cols = pl.ds(pl.multiple_of(i * tile, tile), tile)
+                part[phase, j, :, cols] = jnp.dot(
+                    hidden[...], down_full[s, :, cols], preferred_element_type=f32
+                ).astype(jnp.bfloat16)
+
+            pair_copy(j).start()
+
+        def add_pair(j):
+            pair_copy(j).wait_recv()
+            xs[phase, j] = (part[phase, j, mine, :].astype(f32) + rbuf[phase, j].astype(f32)).astype(jnp.bfloat16)
+            x_copy(j).start()
+
+        def finish(j):
+            x_copy(j).wait_recv()
+            total = xs[phase, j].astype(f32) + xr[phase, j].astype(f32)
+            cols = pl.ds(pl.multiple_of(block(j) * d_loc, 128), d_loc)
+            res[phase, mine, cols] = (base[mine, cols].astype(f32) + 0.5 * total).astype(jnp.bfloat16)
+            final_copy(j, mine).start()
+
+        for j in range(n + 1):
+            if j < n:
+                multiply(j)
+            if j > 0:
+                add_pair(j - 1)
+        for j in range(n):
+            finish(j)
+        for j in range(n):
+            final_copy(j, other).wait_recv()
+
+        def drain():
+            for j in range(n):
+                pair_copy(j).wait_send()
+                x_copy(j).wait_send()
+                final_copy(j, mine).wait_send()
+
+        return drain
+
+    drain_first = branch_sum(0, tok_ref)
+
+    norm_rows(res.at[0], gainm_ref)
+    for off in range(1, n_tp):
+        for s in range(n):
+            pool_copy(off, s, lax.rem(t - off + n_tp, n_tp)).wait_recv()
+    group_width = width // groups
+    row_id = lax.broadcasted_iota(jnp.int32, (n_rows, n_rows), 0)
+    col_id = lax.broadcasted_iota(jnp.int32, (n_rows, n_rows), 1)
+    position = lax.broadcasted_iota(jnp.int32, (n_rows, 1), 0)
+    for k, span in enumerate(pool_spans):
+        low = row_id - span // 2
+        band = jnp.where((col_id >= low) & (col_id < low + span), 1.0, 0.0).astype(jnp.bfloat16)
+        first = jnp.maximum(position - span // 2, 0)
+        last = jnp.minimum(position - span // 2 + span, n_rows)
+        inverse = 1.0 / (last - first).astype(f32)
+        cols = pl.ds(k * group_width, group_width)
+        mean = jnp.dot(band, normed[:, cols], preferred_element_type=f32) * inverse
+        deviation = (mean - normed[:, cols].astype(f32)).astype(jnp.bfloat16)
+        mapped = jnp.dot(deviation, pool_full[k], preferred_element_type=f32) + bias_ref[pl.ds(k, 1), :]
+        amix[:, cols] = (res[0, :, cols].astype(f32) + mapped * scale_ref[:, cols]).astype(jnp.bfloat16)
+
+    norm_rows(amix, gain2_ref)
+
+    @pl.loop(0, f_loc // tile)
+    def _(i):
+        cols = pl.ds(pl.multiple_of(i * tile, tile), tile)
+        gate_proj = jnp.dot(normed[...], gu_full[0, :, cols], preferred_element_type=f32)
+        up_proj = jnp.dot(normed[...], gu_full[1, :, cols], preferred_element_type=f32)
+        hidden[:, cols] = activate(gate_proj, up_proj)
+
+    drain_second = branch_sum(1, amix)
+    out_copy = pltpu.make_async_copy(res.at[1], out_ref, osem)
+    out_copy.start()
+
+    for k in range(n_pieces):
+
+        @pl.when(z < n - 1)
+        def _():
+            own_right(k).wait_send()
+
+        @pl.when(z > 0)
+        def _():
+            own_left(k).wait_send()
+
+    @pl.loop(1, n)
+    def _(d):
+        for k in range(n_pieces):
+
+            def act(s, more, dev):
+                @pl.when(more)
+                def _():
+                    pass_on(k, s, dev).wait_send()
+
+                share(k, s, g).wait_send()
+
+            both_sides(d, act)
+
+    @pl.loop(0, n)
+    def _(s):
+        for off in range(1, n_tp):
+            pool_copy(off, s, t).wait_send()
+
+    drain_first()
+    drain_second()
+    out_copy.wait()
+
+
+def fused_shards(
+    n, n_tp, tokens, gate_weight, up_weight, down_weight, pool_weight, pool_bias, pool_scale,
+    gain_first, gain_mix, gain_second,
+):
+    n_rows, width = tokens.shape
+    d_loc, f_loc = gate_weight.shape
+    groups = pool_weight.shape[1]
+    pool = jnp.swapaxes(pool_weight, 0, 1)
+    bf16, dma, vmem = jnp.bfloat16, pltpu.SemaphoreType.DMA, pltpu.VMEM
+    in_vmem, anywhere = pl.BlockSpec(memory_space=pltpu.VMEM), pl.BlockSpec(memory_space=pl.ANY)
+    half = n_rows // 2
+    return pl.pallas_call(
+        functools.partial(fused_kernel, (n, n_tp)),
+        out_shape=jax.ShapeDtypeStruct((n_rows, width), bf16),
+        in_specs=[in_vmem] + [anywhere] * 4 + [in_vmem] * 5,
+        out_specs=anywhere,
+        scratch_shapes=[
+            vmem((2, n * d_loc, f_loc), bf16),
+            vmem((n, f_loc, d_loc), bf16),
+            vmem((groups, n * pool.shape[1], n_tp * pool.shape[2]), bf16),
+            vmem((2, n_rows, f_loc), jnp.float32),
+            vmem((n_rows, width), bf16),
+            vmem((n_rows, f_loc), bf16),
+            vmem((n_rows, width), bf16),
+            vmem((2, n_rows, width), bf16),
+            vmem((2, n, n_rows, d_loc), bf16),
+            vmem((2, n, half, d_loc), bf16),
+            vmem((2, n, half, d_loc), bf16),
+            vmem((2, n, half, d_loc), bf16),
+            dma((n, 7)), dma((7,)), dma((n, 7)), dma((n, 7)), dma((n, 7)),
+            dma((n_tp - 1, n)), dma((n_tp - 1, n)), dma((4,)),
+            dma((2, n)), dma((2, n)), dma((2, n)), dma((2, n)), dma((2, n)), dma((2, n)), dma,
+        ],
+        compiler_params=pltpu.CompilerParams(
+            collective_id=0, has_side_effects=True, vmem_limit_bytes=60 * 1024 * 1024
+        ),
+    )(
+        tokens, gate_weight, up_weight, down_weight, pool, pool_bias, pool_scale.reshape(1, width),
+        gain_first.reshape(1, width), gain_mix.reshape(1, width), gain_second.reshape(1, width),
+    )
+
+
+def layer(n_grp, n, n_tp, *args):
+    n_rows, width = args[0].shape
+    d_loc, f_loc = args[1].shape
+    pool_rows, _, pool_cols = args[4].shape
+    fits = n_grp == 2 and n_tp == 4 and n % 2 == 0 and n <= 4 and n_rows % 64 == 0
+    fits = fits and d_loc % 256 == 0 and f_loc % 256 == 0 and pool_rows % 32 == 0 and pool_cols % 128 == 0
+    return fused_shards(n, n_tp, *args) if fits else shards(*args)
+
+
 def solution(mesh):
     return jax.shard_map(
-        shards,
+        functools.partial(layer, mesh.shape["grp"], mesh.shape["fs"], mesh.shape["tp"]),
         mesh=mesh,
         in_specs=(
             P(("grp", "fs"), None),

time: 469 us -> 202 us (0.43)
  waiting for transfers between devices: 382 us -> 0 us
  Pallas kernels: 0 us -> 197 us
  matrix products: 45.8 us -> 0 us
  between operations: 13.6 us -> 0.01 us
  blocking collectives: 13 us -> 0 us
  other arithmetic: 11.8 us -> 0 us
    all_gather x4 -> x0, waiting for transfers between devices: 309 us -> none  [the longest x1 99.9 us: shards(): lax.all_gather(gate_weight, 'fs', axis=0, tiled=True)]
    pallas_call x0 -> x1, Pallas kernels: none -> 197 us  [fused_shards(): pl.pallas_call(functools.partial(fused_kernel, (n, n_tp)), out_shape=jax....]
    psum x2 -> x0, waiting for transfers between devices: 70.2 us -> none  [the longest x1 42.5 us: shards(): lax.psum(jnp.dot(second_hidden, second_down, preferred_element_type=jnp.f...]
    dot_general x8 -> x0, matrix products: 45.8 us -> none  [the longest x2 12 us: ffn_hidden(): gate_proj = jnp.dot(normed, gate_full, preferred_element_type=jnp.float32)]
    all_gather x1 -> x0, blocking collectives: 13 us -> none  [shards(): lax.all_gather(pool_weight, 'fs', axis=0, tiled=True)]
    convert_element_type x6 -> x0, other arithmetic: 6.27 us -> none  [the longest x1 3.22 us: shards(): (after_mix.astype(jnp.float32) + 0.5 * second_branch).astype(jnp.bfloat16)]
    reduce_sum x3 -> x0, other arithmetic: 5.52 us -> none  [rms_scale(): jnp.mean(fvalues * fvalues, axis=-1, keepdims=True) + eps]
  transfers between devices with their start and end apart: 6 -> 0, of which waited for: 6 -> 0; matrix products, arithmetic and copies ran while one was open for 3% -> 0% of each run, Pallas kernels for 0% -> 0%
where the time goes in v1:
time: 202 us; the launch traced here: 201 us
  Pallas kernels  197 us (98%)
  local copies, waits for them, and re-layouts  4.3 us (2%)
    pallas_call x1, Pallas kernels, fused_shards(): pl.pallas_call(functools.partial(fused_kernel, (n, n_tp)), out_shape=jax....  197 us
    unnamed x2, local copies, waits for them, and re-layouts  4.3 us

profile of v1, /device:TPU:1, one launch (start us, length us, event | category | flops | bytes accessed | tf_op | source)
XLA Modules:
  0.0 201.4 jit_solution(6865306320474216045)
XLA Ops:
  0.0 1.6 copy.13
  1.6 197.1 %shard_map.100 = bf16[384,2048]{1,0:T(8,128)(2,1)} custom-call(bf16[384,2048]{1,0:T(8,128)(2,1)} %tok_ref.1, bf16[512,1280]{1,0:T(8,128)(2,1)} %gate_ref.1, bf16[512,1280]{1,0:T(8,128)(2,1)} %up_ref.1, bf16[1280,512]{1,0:T(8,128)(2,1)} %down_ref.1, bf16[4,128,128]{2,1,0:T(8,128)(2,1)} %bitcast.7, f32[4,512]{1,0:T(4,128)} %bias_ref.1, f32[1,2048]{1,0:T(1,128)} %bitcast.8, ...), custom_call_target="tpu_custom_call" | custom-call | tf_op jit(solution)/shard_map/pallas_call | solution.py:442
  198.7 2.7 %copy.15 = bf16[384,2048]{1,0:T(8,128)(2,1)} copy(bf16[384,2048]{1,0:T(8,128)(2,1)} %shard_map.100) | data formatting | bytes 3145728

commit v2 on v1

--- a/solution.py
+++ b/solution.py
@@ -110,6 +110,7 @@
     d_loc, f_loc = gate_ref.shape
     groups, pool_rows, pool_cols = pool_ref.shape
     half_rows = n_rows // 2
+    block_cols = d_loc // 2
     f32 = jnp.float32
 
     def remote(src, dst, s_sem, r_sem, dev):
@@ -136,18 +137,20 @@
 
     pl.semaphore_wait(barrier, n_tp + jnp.minimum(z, 1) + jnp.minimum(n - 1 - z, 1))
 
-    pieces = [("pool", 0, 1)] + [(name, c, 2) for name in ("gate", "up", "down") for c in range(2)]
+    pieces = [("pool", 0, 1)] + [(name, c, 4) for name in ("gate", "up", "down") for c in range(4)]
     n_pieces = len(pieces)
 
     def rows_of(name, half, c, count):
-        total = {"pool": pool_rows, "gate": d_loc, "up": d_loc, "down": f_loc}[name]
+        if name == "down":
+            return c * (f_loc // count), f_loc // count, f_loc
+        total = {"pool": pool_rows, "gate": d_loc, "up": d_loc}[name]
         size = total // (2 * count)
         return half * (total // 2) + c * size, size, total
 
     def region(name, s, half, c, count):
         start, size, total = rows_of(name, half, c, count)
         if name == "down":
-            return down_full.at[s, pl.ds(pl.multiple_of(start, 16), size), :]
+            return down_full.at[s, half, pl.ds(start, size), :]
         rows = pl.ds(pl.multiple_of(s * total + start, 16), size)
         if name == "pool":
             return pool_full.at[:, rows, pl.ds(pl.multiple_of(t * pool_cols, 128), pool_cols)]
@@ -155,10 +158,12 @@
 
     def source(name, half, c, count):
         start, size, _ = rows_of(name, half, c, count)
+        if name == "down":
+            return down_ref.at[pl.ds(start, size), pl.ds(pl.multiple_of(half * block_cols, 128), block_cols)]
         rows = pl.ds(pl.multiple_of(start, 16), size)
         if name == "pool":
             return pool_ref.at[:, rows, :]
-        return {"gate": gate_ref, "up": up_ref, "down": down_ref}[name].at[rows, :]
+        return {"gate": gate_ref, "up": up_ref}[name].at[rows, :]
 
     def own_right(k):
         name, c, count = pieces[k]
@@ -196,7 +201,8 @@
         pltpu.make_async_copy(pool_ref, own_pool, lsem.at[0]),
         pltpu.make_async_copy(gate_ref, gu_full.at[0, own_rows, :], lsem.at[1]),
         pltpu.make_async_copy(up_ref, gu_full.at[1, own_rows, :], lsem.at[2]),
-        pltpu.make_async_copy(down_ref, down_full.at[z], lsem.at[3]),
+        pltpu.make_async_copy(down_ref.at[:, pl.ds(0, block_cols)], down_full.at[z, 0], lsem.at[3]),
+        pltpu.make_async_copy(down_ref.at[:, pl.ds(block_cols, block_cols)], down_full.at[z, 1], lsem.at[4]),
     ]
     for copy in local:
         copy.start()
@@ -247,9 +253,9 @@
         def _():
             act(z + d, z > 0, left)
 
-    def relay(name, d):
+    def relay(name, d, only=None):
         for k in range(n_pieces):
-            if pieces[k][0] != name:
+            if pieces[k][0] != name or only not in (None, pieces[k][1]):
                 continue
 
             def act(s, more, dev):
@@ -280,7 +286,7 @@
         settle("up", s)
         add_shard(1, s)
 
-    @pl.loop(1, n)
+    @pl.loop(1, n - 1)
     def _(d):
         relay("pool", d)
         relay("gate", d)
@@ -290,6 +296,15 @@
         relay("down", d)
         both_sides(d, settle_up)
 
+    relay("pool", n - 1)
+    relay("gate", n - 1)
+    both_sides(n - 1, settle_pool)
+    relay("up", n - 1)
+    both_sides(n - 1, settle_gate)
+    relay("down", n - 1, 0)
+    both_sides(n - 1, settle_up)
+    relay("down", n - 1, 1)
+
     def activate(gate_proj, up_proj):
         return (gate_proj / (1.0 + jnp.exp(-gate_proj)) * up_proj).astype(jnp.bfloat16)
 
@@ -302,9 +317,15 @@
     mine = pl.ds(pl.multiple_of(core * half_rows, 16), half_rows)
     other = pl.ds(pl.multiple_of((1 - core) * half_rows, 16), half_rows)
 
+    n_blocks = 2 * n
+
     def branch_sum(phase, base):
-        def block(j):
-            return lax.rem(z + turn * j + n, n)
+        def place(j):
+            return lax.rem(z + turn * (j // 2) + n, n), g if j % 2 == 0 else 1 - g
+
+        def columns(j):
+            s, half = place(j)
+            return pl.ds(pl.multiple_of(s * d_loc + half * block_cols, 128), block_cols)
 
         def pair_copy(j):
             return remote(part.at[phase, j, other, :], rbuf.at[phase, j], csend.at[phase, j], crecv.at[phase, j], mate)
@@ -313,21 +334,18 @@
             return remote(xs.at[phase, j], xr.at[phase, j], xsend.at[phase, j], xrecv.at[phase, j], x_peer)
 
         def final_copy(j, rows):
-            there = res.at[phase, rows, pl.ds(pl.multiple_of(block(j) * d_loc, 128), d_loc)]
+            there = res.at[phase, rows, columns(j)]
             return remote(there, there, fsend.at[phase, j], frecv.at[phase, j], mate)
 
         def multiply(j):
-            s = block(j)
-            if phase == 0 and j > 0:
+            s, half = place(j)
+            if phase == 0 and j in (2, 3):
+                relay("down", n - 1, j)
+            if phase == 0 and j >= 2 and j % 2 == 1:
                 settle("down", s)
-
-            @pl.loop(0, d_loc // tile)
-            def _(i):
-                cols = pl.ds(pl.multiple_of(i * tile, tile), tile)
-                part[phase, j, :, cols] = jnp.dot(
-                    hidden[...], down_full[s, :, cols], preferred_element_type=f32
-                ).astype(jnp.bfloat16)
-
+            part[phase, j] = jnp.dot(
+                hidden[...], down_full[s, half], preferred_element_type=f32
+            ).astype(jnp.bfloat16)
             pair_copy(j).start()
 
         def add_pair(j):
@@ -338,22 +356,26 @@
         def finish(j):
             x_copy(j).wait_recv()
             total = xs[phase, j].astype(f32) + xr[phase, j].astype(f32)
-            cols = pl.ds(pl.multiple_of(block(j) * d_loc, 128), d_loc)
+            cols = columns(j)
             res[phase, mine, cols] = (base[mine, cols].astype(f32) + 0.5 * total).astype(jnp.bfloat16)
             final_copy(j, mine).start()
 
-        for j in range(n + 1):
-            if j < n:
+        early = n_blocks // 2 if phase == 0 else 0
+        for j in range(n_blocks + 1):
+            if j == n_blocks - 1:
+                for done in range(early):
+                    finish(done)
+            if j < n_blocks:
                 multiply(j)
             if j > 0:
                 add_pair(j - 1)
-        for j in range(n):
+        for j in range(early, n_blocks):
             finish(j)
-        for j in range(n):
+        for j in range(n_blocks):
             final_copy(j, other).wait_recv()
 
         def drain():
-            for j in range(n):
+            for j in range(n_blocks):
                 pair_copy(j).wait_send()
                 x_copy(j).wait_send()
                 final_copy(j, mine).wait_send()
@@ -446,20 +468,20 @@
         out_specs=anywhere,
         scratch_shapes=[
             vmem((2, n * d_loc, f_loc), bf16),
-            vmem((n, f_loc, d_loc), bf16),
+            vmem((n, 2, f_loc, d_loc // 2), bf16),
             vmem((groups, n * pool.shape[1], n_tp * pool.shape[2]), bf16),
             vmem((2, n_rows, f_loc), jnp.float32),
             vmem((n_rows, width), bf16),
             vmem((n_rows, f_loc), bf16),
             vmem((n_rows, width), bf16),
             vmem((2, n_rows, width), bf16),
-            vmem((2, n, n_rows, d_loc), bf16),
-            vmem((2, n, half, d_loc), bf16),
-            vmem((2, n, half, d_loc), bf16),
-            vmem((2, n, half, d_loc), bf16),
-            dma((n, 7)), dma((7,)), dma((n, 7)), dma((n, 7)), dma((n, 7)),
-            dma((n_tp - 1, n)), dma((n_tp - 1, n)), dma((4,)),
-            dma((2, n)), dma((2, n)), dma((2, n)), dma((2, n)), dma((2, n)), dma((2, n)), dma,
+            vmem((2, 2 * n, n_rows, d_loc // 2), bf16),
+            vmem((2, 2 * n, half, d_loc // 2), bf16),
+            vmem((2, 2 * n, half, d_loc // 2), bf16),
+            vmem((2, 2 * n, half, d_loc // 2), bf16),
+            dma((n, 13)), dma((13,)), dma((n, 13)), dma((n, 13)), dma((n, 13)),
+            dma((n_tp - 1, n)), dma((n_tp - 1, n)), dma((5,)),
+            *[dma((2, 2 * n))] * 6, dma,
         ],
         compiler_params=pltpu.CompilerParams(
             collective_id=0, has_side_effects=True, vmem_limit_bytes=60 * 1024 * 1024
@@ -475,7 +497,7 @@
     d_loc, f_loc = args[1].shape
     pool_rows, _, pool_cols = args[4].shape
     fits = n_grp == 2 and n_tp == 4 and n % 2 == 0 and n <= 4 and n_rows % 64 == 0
-    fits = fits and d_loc % 256 == 0 and f_loc % 256 == 0 and pool_rows % 32 == 0 and pool_cols % 128 == 0
+    fits = fits and d_loc % 512 == 0 and f_loc % 256 == 0 and pool_rows % 32 == 0 and pool_cols % 128 == 0
     return fused_shards(n, n_tp, *args) if fits else shards(*args)
 
 

time: 202 us -> 194 us (0.960)
  Pallas kernels: 197 us -> 190 us
    pallas_call x1, Pallas kernels: 197 us -> 190 us  [fused_shards(): pl.pallas_call(functools.partial(fused_kernel, (n, n_tp)), out_shape=jax....]
where the time goes in v2:
time: 194 us
  Pallas kernels  190 us (98%)
  local copies, waits for them, and re-layouts  4.3 us (2%)
    pallas_call x1, Pallas kernels, fused_shards(): pl.pallas_call(functools.partial(fused_kernel, (n, n_tp)), out_shape=jax....  190 us
    unnamed x2, local copies, waits for them, and re-layouts  4.3 us

profile of v2, /device:TPU:1, one launch (start us, length us, event | category | flops | bytes accessed | tf_op | source)
XLA Modules:
  0.0 193.8 jit_solution(6438378146137283471)
XLA Ops:
  0.0 1.6 copy.13
  1.6 189.5 %shard_map.100 = bf16[384,2048]{1,0:T(8,128)(2,1)} custom-call(bf16[384,2048]{1,0:T(8,128)(2,1)} %tok_ref.1, bf16[512,1280]{1,0:T(8,128)(2,1)} %gate_ref.1, bf16[512,1280]{1,0:T(8,128)(2,1)} %up_ref.1, bf16[1280,512]{1,0:T(8,128)(2,1)} %down_ref.1, bf16[4,128,128]{2,1,0:T(8,128)(2,1)} %bitcast.7, f32[4,512]{1,0:T(4,128)} %bias_ref.1, f32[1,2048]{1,0:T(1,128)} %bitcast.8, ...), custom_call_target="tpu_custom_call" | custom-call | tf_op jit(solution)/shard_map/pallas_call | solution.py:464
  191.1 2.7 %copy.15 = bf16[384,2048]{1,0:T(8,128)(2,1)} copy(bf16[384,2048]{1,0:T(8,128)(2,1)} %shard_map.100) | data formatting | bytes 3145728

commit v3 on v2

--- a/solution.py
+++ b/solution.py
@@ -301,9 +301,8 @@
     both_sides(n - 1, settle_pool)
     relay("up", n - 1)
     both_sides(n - 1, settle_gate)
+    both_sides(n - 1, settle_up)
     relay("down", n - 1, 0)
-    both_sides(n - 1, settle_up)
-    relay("down", n - 1, 1)
 
     def activate(gate_proj, up_proj):
         return (gate_proj / (1.0 + jnp.exp(-gate_proj)) * up_proj).astype(jnp.bfloat16)
@@ -339,8 +338,8 @@
 
         def multiply(j):
             s, half = place(j)
-            if phase == 0 and j in (2, 3):
-                relay("down", n - 1, j)
+            if phase == 0 and j in (1, 3, 5):
+                relay("down", n - 1, (j + 1) // 2)
             if phase == 0 and j >= 2 and j % 2 == 1:
                 settle("down", s)
             part[phase, j] = jnp.dot(

time: 194 us -> 194 us (level)
  no operation moved by 1% of the time
where the time goes in v3:
time: 194 us; the launch traced here: 193 us
  Pallas kernels  189 us (97%)
  local copies, waits for them, and re-layouts  4.3 us (2%)
    pallas_call x1, Pallas kernels, fused_shards(): pl.pallas_call(functools.partial(fused_kernel, (n, n_tp)), out_shape=jax....  189 us
    unnamed x2, local copies, waits for them, and re-layouts  4.3 us

profile of v3, /device:TPU:1, one launch (start us, length us, event | category | flops | bytes accessed | tf_op | source)
XLA Modules:
  0.0 193.2 jit_solution(11247294013662869065)
XLA Ops:
  0.0 1.6 copy.13
  1.6 188.9 %shard_map.100 = bf16[384,2048]{1,0:T(8,128)(2,1)} custom-call(bf16[384,2048]{1,0:T(8,128)(2,1)} %tok_ref.1, bf16[512,1280]{1,0:T(8,128)(2,1)} %gate_ref.1, bf16[512,1280]{1,0:T(8,128)(2,1)} %up_ref.1, bf16[1280,512]{1,0:T(8,128)(2,1)} %down_ref.1, bf16[4,128,128]{2,1,0:T(8,128)(2,1)} %bitcast.7, f32[4,512]{1,0:T(4,128)} %bias_ref.1, f32[1,2048]{1,0:T(1,128)} %bitcast.8, ...), custom_call_target="tpu_custom_call" | custom-call | tf_op jit(solution)/shard_map/pallas_call | solution.py:463
  190.4 2.7 %copy.15 = bf16[384,2048]{1,0:T(8,128)(2,1)} copy(bf16[384,2048]{1,0:T(8,128)(2,1)} %shard_map.100) | data formatting | bytes 3145728
